TPU v7x, 32 devices: a whole 2x2x4 slice. The times are simulated.
32 devices in a mesh: sp: 16 (over z, y, x), tp: 2 (over core).
Axes of the slice: x: 2, y: 2, z: 4, core: 2. Of those that a mesh axis runs over, the one named last changes fastest.
Arguments:
- residual: bfloat16 [2048, 2048], P('sp'), may hold values from -6 to 6
- query_nope: bfloat16 [2048, 8, 128], P('sp', 'tp'), may hold values from -6 to 6
- query_rope: bfloat16 [2048, 8, 64], P('sp', 'tp'), may hold values from -64 to 64
- latent: bfloat16 [2048, 256], P('sp'), may hold values from -6 to 6
- rope_key: bfloat16 [2048, 64], P('sp'), may hold values from -64 to 64
- kv_gain: bfloat16 [256], replicated, may hold values from 0.099609375 to 1.8984375
- key_up: bfloat16 [256, 8, 128], replicated, may hold values from -0.375 to 0.375
- value_up: bfloat16 [256, 8, 128], replicated, may hold values from -0.375 to 0.375
- out_weight: bfloat16 [1024, 2048], P('tp'), may hold values from -0.1875 to 0.1875
- post_gain: bfloat16 [2048], replicated, may hold values from 0.099609375 to 1.8984375
- pre_gain: bfloat16 [2048], replicated, may hold values from 0.099609375 to 1.8984375
- ffn_gain: bfloat16 [2048], replicated, may hold values from 0.099609375 to 1.8984375
- up_value: bfloat16 [2048, 5632], P('sp', 'tp'), may hold values from -0.125 to 0.125
- up_gate: bfloat16 [2048, 5632], P('sp', 'tp'), may hold values from -0.125 to 0.125
- conv_value: bfloat16 [3, 5632], replicated, may hold values from -3.5 to 3.5
- conv_gate: bfloat16 [3, 5632], replicated, may hold values from -3.5 to 3.5
- down_weight: bfloat16 [5632, 2048], P('tp', 'sp'), may hold values from -0.078125 to 0.078125
Outputs:
- layer_out: bfloat16 [2048, 2048], P(('sp', 'tp'))
All inputs are finite; a program needn't handle non-finite values.
Results may differ from a plain program's by a relative error of at most 0.02.
Values may be sent and summed in bfloat16 or wider, within the bound.
A program may use at most 128 MiB of HBM per device.

v0:
```python
import jax
import jax.numpy as jnp
from jax import lax
from jax.sharding import PartitionSpec as P

GRID = 64


epsilon = 1e-06
rope_base = 10000.0


def extended(x, sides, width):
    for axis, dim in sides:
        size, length = (lax.axis_size(axis), x.shape[dim])
        up = [(i, (i + 1) % size) for i in range(size - 1)]
        down = [(j, i) for i, j in up]
        last = lax.slice_in_dim(x, length - width, length, axis=dim)
        initial = lax.slice_in_dim(x, 0, width, axis=dim)
        before = lax.ppermute(last, axis, up)
        after = lax.ppermute(initial, axis, down)
        x = jnp.concatenate([before, x, after], axis=dim)
    return x


def rms_norm(values, gain):
    return (
        values
        * lax.rsqrt(jnp.mean(values * values, axis=-1, keepdims=True) + epsilon)
        * gain.astype(jnp.float32)
    )


def widened(values):
    return lax.optimization_barrier(values.astype(jnp.bfloat16)).astype(jnp.float32)


def rotate(values, positions):
    pair_count = values.shape[-1] // 4
    frequency = rope_base ** (-jnp.arange(pair_count, dtype=jnp.float32) / pair_count)
    grid_rows = (positions // GRID).astype(jnp.float32)
    grid_cols = (positions % GRID).astype(jnp.float32)
    angles = jnp.stack([grid_rows, grid_cols], axis=-1)[:, :, None] * frequency
    table_shape = (angles.shape[0],) + (1,) * (values.ndim - 2) + angles.shape[1:]
    cosine = jnp.cos(angles).reshape(table_shape)
    sine = jnp.sin(angles).reshape(table_shape)
    halves = values.reshape(values.shape[:-1] + (2, 2, pair_count))
    leading = halves[..., 0, :]
    trailing = halves[..., 1, :]
    turned = jnp.stack(
        [leading * cosine - trailing * sine, trailing * cosine + leading * sine], axis=-2
    )
    return turned.reshape(values.shape)


def body(
    residual,
    query_nope,
    query_rope,
    latent,
    rope_key,
    kv_gain,
    key_up,
    value_up,
    out_weight,
    post_gain,
    pre_gain,
    ffn_gain,
    up_value,
    up_gate,
    conv_value,
    conv_gate,
    down_weight,
):
    tok_rows = residual.shape[0]
    heads_dev = query_nope.shape[1]
    value_width = value_up.shape[2]
    tp_index = lax.axis_index("tp")
    positions = lax.axis_index("sp") * tok_rows + jnp.arange(tok_rows, dtype=jnp.int32)
    score_scale = (query_nope.shape[2] + query_rope.shape[2]) ** (-0.5)
    normed = rms_norm(latent.astype(jnp.float32), kv_gain).astype(jnp.bfloat16)
    key_turn = rotate(rope_key.astype(jnp.float32), positions).astype(jnp.bfloat16)
    query_turn = rotate(query_rope.astype(jnp.float32), positions).astype(jnp.bfloat16)
    key_local = lax.dynamic_slice_in_dim(key_up, tp_index * heads_dev, heads_dev, 1)
    value_local = lax.dynamic_slice_in_dim(value_up, tp_index * heads_dev, heads_dev, 1)
    pieces = (
        lax.all_gather(normed, "sp", axis=0, tiled=True),
        lax.all_gather(key_turn, "sp", axis=0, tiled=True),
    )
    keys_nope = jnp.einsum(
        "nc,chd->nhd", pieces[0], key_local, preferred_element_type=jnp.float32
    ).astype(jnp.bfloat16)
    values_part = jnp.einsum(
        "nc,chd->nhd", pieces[0], value_local, preferred_element_type=jnp.float32
    ).astype(jnp.bfloat16)
    row_max = jnp.full((heads_dev, tok_rows), -1e30, jnp.float32)
    scores = (
        jnp.einsum("qhd,khd->hqk", query_nope, keys_nope, preferred_element_type=jnp.float32)
        + jnp.einsum("qhd,kd->hqk", query_turn, pieces[1], preferred_element_type=jnp.float32)
    ) * score_scale
    new_max = jnp.maximum(row_max, jnp.max(scores, axis=-1))
    weights = jnp.exp(scores - new_max[:, :, None])
    totals = jnp.sum(weights, axis=-1)
    weighted = jnp.einsum(
        "hqk,khd->hqd",
        weights.astype(jnp.bfloat16),
        values_part,
        preferred_element_type=jnp.float32,
    )
    attended = (weighted / totals[:, :, None]).astype(jnp.bfloat16)
    attended = jnp.transpose(attended, (1, 0, 2)).reshape(tok_rows, heads_dev * value_width)
    row_share = tok_rows // lax.axis_size("tp")
    summed = lax.psum_scatter(
        jnp.dot(attended, out_weight, preferred_element_type=jnp.float32).astype(jnp.bfloat16),
        "tp",
        scatter_dimension=0,
        tiled=True,
    ).astype(jnp.float32)
    own_rows = lax.dynamic_slice_in_dim(residual, tp_index * row_share, row_share, 0).astype(
        jnp.float32
    )
    stream_wide = widened(own_rows + rms_norm(widened(summed), post_gain))
    inputs = lax.all_gather(
        rms_norm(stream_wide, pre_gain).astype(jnp.bfloat16), "tp", axis=0, tiled=True
    )
    ff_dev = up_value.shape[1]
    up_joined = jnp.concatenate([up_value, up_gate], axis=1)
    up_whole = lax.all_gather(up_joined, "sp", axis=0, tiled=True)
    up_pair = jnp.dot(inputs, up_whole, preferred_element_type=jnp.float32).astype(jnp.bfloat16)
    padded = extended(up_pair, (("sp", 0),), 1).astype(jnp.float32)
    channel_start = tp_index * ff_dev
    conv_taps = jnp.concatenate(
        [
            lax.dynamic_slice_in_dim(conv_value, channel_start, ff_dev, 1),
            lax.dynamic_slice_in_dim(conv_gate, channel_start, ff_dev, 1),
        ],
        axis=1,
    ).astype(jnp.float32)
    mixed_conv = (
        padded[:-2] * conv_taps[0] + padded[1:-1] * conv_taps[1] + padded[2:] * conv_taps[2]
    )
    hidden = (jax.nn.silu(mixed_conv[:, ff_dev:]) * mixed_conv[:, :ff_dev]).astype(jnp.bfloat16)
    down_whole = lax.all_gather(down_weight, "sp", axis=1, tiled=True)
    down_terms = jnp.dot(hidden, down_whole, preferred_element_type=jnp.float32)
    reduced = lax.psum_scatter(
        down_terms.astype(jnp.bfloat16), "tp", scatter_dimension=0, tiled=True
    ).astype(jnp.float32)
    return (stream_wide + rms_norm(widened(reduced), ffn_gain)).astype(jnp.bfloat16)


def solution(mesh):
    placed = (
        P("sp", None),
        P("sp", "tp", None),
        P("sp", "tp", None),
        P("sp", None),
        P("sp", None),
        P(),
        P(),
        P(),
        P("tp", None),
        P(),
        P(),
        P(),
        P("sp", "tp"),
        P("sp", "tp"),
        P(),
        P(),
        P("tp", "sp"),
    )
    return jax.shard_map(
        body, mesh=mesh, in_specs=placed, out_specs=P(("sp", "tp"), None), check_vma=False
    )
```

profile of v0, /device:TPU:0, one launch (start us, length us, event | category | flops | bytes accessed | tf_op | source)
XLA Modules:
  0.0 553.0 jit_solution(2200279591683789855)
XLA Ops:
  6.5 0.0 copy-start
  6.5 1.1 fusion.40
  7.6 0.7 convert_element_type.108
  8.3 1.6 fusion.42
  9.9 0.0 all-gather.4.cloned.1.call-update
  9.9 0.0 reduce-scatter.3.cloned.1.call-start
  9.9 0.9 convert.19
  10.8 0.7 convert.18
  11.6 0.1 fusion.51
  11.7 0.1 multiply_cosine_fusion
  11.9 44.1 %all_gather.16 = bf16[2048,64]{0,1:T(8,128)(2,1)S(1)} all-gather(bf16[128,64]{0,1:T(8,128)(2,1)S(1)} %bitcast.41), channel_id=1, replica_groups=mesh['sp'=16,'tp'=2] {'sp'}, dimensions={0}, use_global_device_ids=true | all-gather | bytes 278528 | tf_op jit(solution)/shard_map/all_gather | solution.py:88
  56.0 1.5 constant_dynamic-slice_fusion.2
  57.5 10.8 %all-gather.4.cloned.1.call-done = bf16[2048,256]{1,0:T(8,128)(2,1)} async-done(((bf16[128,256]{1,0:T(8,128)(2,1)}), bf16[2048,256]{1,0:T(8,128)(2,1)}) %all-gather.4.cloned.1.call-update) | async-done | bytes 1048592 | tf_op jit(solution)/shard_map/all_gather | solution.py:87
  68.3 4.4 fusion.8
  72.7 2.9 fusion.58
  75.7 1.9 copy-done.1
  77.6 0.6 fusion.1
  78.2 4.3 fusion.16
  82.5 2.3 convolution_convert_fusion.4
  84.8 0.0 reduce-scatter.3.cloned.1.call-update
  84.8 0.0 all-gather.6.cloned.1.call-start
  84.8 1.2 pad_maximum_fusion
  86.0 0.0 all-gather.6.cloned.1.call-update
  86.1 0.0 all-gather.8.cloned.1.call-start
  86.1 0.5 all-gather.8.cloned.1.call-update
  86.7 0.0 reduce-scatter.5.cloned.1.call-start
  86.7 0.8 constant_dynamic-slice_fusion
  87.5 4.2 reduce-scatter.3.cloned.1.call-done
  91.7 1.1 fusion.25
  92.8 1.2 fusion.28
  94.0 0.2 fusion.31
  94.2 0.1 fusion.33
  94.3 2.2 all_gather.17
  96.5 249.5 %all-gather.6.cloned.1.call-done = bf16[2048,5632]{1,0:T(8,128)(2,1)} async-done(((bf16[128,5632]{1,0:T(8,128)(2,1)}), bf16[2048,5632]{1,0:T(8,128)(2,1)}) %all-gather.6.cloned.1.call-update) | async-done | bytes 23068688 | tf_op jit(solution)/shard_map/all_gather | solution.py:128
  346.1 10.7 %convolution_convert_fusion = bf16[128,5632]{1,0:T(8,128)(2,1)S(1)} fusion(bf16[128,2048]{1,0:T(8,128)(2,1)S(1)} %all_gather.17, bf16[2048,5632]{1,0:T(8,128)(2,1)} %all-gather.6.cloned.1.call-done), kind=kOutput, calls=%fused_computation | convolution fusion | flops 2953510912 | bytes 25034752 | tf_op jit(solution)/shard_map/dot_general | solution.py:129
  356.8 3.4 collective-permute-start
  360.2 1.5 collective-permute-start.1
  361.7 0.2 convert_reduce_fusion.1
  361.9 0.2 collective-permute-done
  362.1 4.4 collective-permute-done.1
  366.5 0.4 maximum_convert_fusion
  366.9 2.4 fusion.3
  369.4 160.2 %all-gather.8.cloned.1.call-done = bf16[2816,2048]{1,0:T(8,128)(2,1)} async-done(((bf16[2816,128]{1,0:T(8,128)(2,1)}), bf16[2816,2048]{1,0:T(8,128)(2,1)}) %all-gather.8.cloned.1.call-update) | async-done | bytes 11534352 | tf_op jit(solution)/shard_map/all_gather | solution.py:143
  529.5 7.7 %convolution_convert_fusion.3 = bf16[128,2048]{1,0:T(8,128)(2,1)} fusion(bf16[2816,2048]{1,0:T(8,128)(2,1)} %all-gather.8.cloned.1.call-done, f32[128,5632]{1,0:T(8,128)} %fusion.3), kind=kOutput, calls=%fused_computation.13 | convolution fusion | flops 1478819840 | bytes 14942208 | tf_op jit(solution)/shard_map/dot_general | solution.py:144
  537.2 0.0 reduce-scatter.5.cloned.1.call-update
  537.3 6.2 %reduce-scatter.5.cloned.1.call-done = bf16[64,2048]{1,0:T(8,128)(2,1)} async-done(((bf16[128,2048]{1,0:T(8,128)(2,1)}), bf16[64,2048]{1,0:T(8,128)(2,1)}) %reduce-scatter.5.cloned.1.call-update) | async-done | bytes 262160 | tf_op jit(solution)/shard_map/reduce_scatter | solution.py:145
  543.5 1.1 fusion.29
  544.6 1.8 fusion.34
  (30 shorter events, 0.2 us)
Async XLA Ops:
  6.5 75.9 %copy-start = (bf16[512,2048]{1,0:T(8,128)(2,1)S(1)}, bf16[512,2048]{1,0:T(8,128)(2,1)}, u32[]{:S(2)}) copy-start(bf16[512,2048]{1,0:T(8,128)(2,1)} %param.25) | copy-start | bytes 6291460
  6.5 61.8 %all-gather.4.cloned.1.call-start = ((), (), s32[]{:S(2)}) async-start(), calls=%async_computation.2 | async-start | bytes 1114112 | tf_op jit(solution)/shard_map/all_gather | solution.py:87
  9.9 81.8 %reduce-scatter.3.cloned.1.call-start = ((), (), s32[]{:S(2)}) async-start(), calls=%async_computation.3 | async-start | bytes 786432 | tf_op jit(solution)/shard_map/reduce_scatter | solution.py:113
  75.7 1.9 copy-start.1
  75.7 2.5 copy-start.2
  82.5 2.4 copy-start.3
  82.5 2.4 copy-start.4
  84.7 2.0 copy-start.5
  84.8 2.0 copy-start.6
  84.8 261.3 %all-gather.6.cloned.1.call-start = ((), (), s32[]{:S(2)}) async-start(), calls=%async_computation.4 | async-start | bytes 24510464 | tf_op jit(solution)/shard_map/all_gather | solution.py:128
  86.1 443.5 %all-gather.8.cloned.1.call-start = ((), (), s32[]{:S(2)}) async-start(), calls=%async_computation.5 | async-start | bytes 12255232 | tf_op jit(solution)/shard_map/all_gather | solution.py:143
  86.7 456.9 %reduce-scatter.5.cloned.1.call-start = ((), (), s32[]{:S(2)}) async-start(), calls=%async_computation.6 | async-start | bytes 786432 | tf_op jit(solution)/shard_map/reduce_scatter | solution.py:145
  356.8 5.3 collective-permute-start
  360.2 6.3 %collective-permute-start.1 = (bf16[1,5632]{1,0:T(2,128)(2,1)S(1)}, bf16[1,5632]{1,0:T(2,128)(2,1)S(1)}, u32[]{:S(2)}, u32[]{:S(2)}) collective-permute-start(bf16[1,5632]{1,0:T(2,128)(2,1)S(1)} %get-tuple-element.9), channel_id=1, source_target_pairs={{2,0},{4,2},{6,4},{8,6},{10,8},{12,10},{14,12},{16,14},{18,16},{20... | collective-permute-start | bytes 33800 | tf_op jit(solution)/shard_map/ppermute | solution.py:21
  369.4 167.9 %copy-start.7 = (bf16[2048]{0:T(1024)(128)(2,1)S(1)}, bf16[2048]{0:T(1024)(128)(2,1)}, u32[]{:S(2)}) copy-start(bf16[2048]{0:T(1024)(128)(2,1)} %param.28) | copy-start | bytes 12292
Sparse Core Ops, SparseCore 0:
  10.1 58.1 all-gather.3
  84.9 6.7 reduce-scatter.2
  94.4 251.6 all-gather.5
  348.6 180.8 all-gather.7
  537.4 6.0 reduce-scatter.4
where the time goes:
time: 554 us; the launch traced here: 553 us
  waiting for transfers between devices  436 us (79%)
  blocking collectives  46.3 us (8%)
  matrix products  32.3 us (6%)
  other arithmetic  15.6 us (3%)
  between operations  13.4 us (2%)
    all_gather x1, waiting for transfers between devices, body(): up_whole = lax.all_gather(up_joined, 'sp', axis=0, tiled=True)  250 us
    all_gather x1, waiting for transfers between devices, body(): down_whole = lax.all_gather(down_weight, 'sp', axis=1, tiled=True)  160 us
    all_gather x1, blocking collectives, body(): lax.all_gather(key_turn, 'sp', axis=0, tiled=True)  44.1 us
  transfers between devices with their start and end apart: 7, of which 7 were waited for; matrix products, arithmetic and copies ran while one was open for 4% of the time, Pallas kernels for 0%

commit v1 on v0

--- a/solution.py
+++ b/solution.py
@@ -51,6 +51,35 @@
         [leading * cosine - trailing * sine, trailing * cosine + leading * sine], axis=-2
     )
     return turned.reshape(values.shape)
+
+
+def feed_by_units(
+    own_inputs, stream_wide, up_value, up_gate, conv_value, conv_gate, down_weight, ffn_gain
+):
+    sp_size = lax.axis_size("sp")
+    ff_dev = up_value.shape[1]
+    unit = ff_dev // sp_size
+    first_unit = lax.axis_index("tp") * ff_dev + lax.axis_index("sp") * unit
+    up_pair = jnp.stack(
+        [up_value.reshape(-1, sp_size, unit), up_gate.reshape(-1, sp_size, unit)], axis=0
+    )
+    up_mine = lax.all_to_all(up_pair, "sp", split_axis=2, concat_axis=1, tiled=True)[:, :, 0]
+    down_mine = lax.all_to_all(down_weight, "sp", split_axis=0, concat_axis=1, tiled=True)
+    inputs = lax.all_gather(own_inputs, ("sp", "tp"), axis=0, tiled=True)
+
+    def conved(weight, taps):
+        rows = jnp.dot(inputs, weight, preferred_element_type=jnp.float32).astype(jnp.bfloat16)
+        padded = jnp.pad(rows, ((1, 1), (0, 0))).astype(jnp.float32)
+        taps = lax.dynamic_slice_in_dim(taps, first_unit, unit, 1).astype(jnp.float32)
+        return padded[:-2] * taps[0] + padded[1:-1] * taps[1] + padded[2:] * taps[2]
+
+    hidden = jax.nn.silu(conved(up_mine[1], conv_gate)) * conved(up_mine[0], conv_value)
+    terms = jnp.dot(
+        hidden.astype(jnp.bfloat16), down_mine, preferred_element_type=jnp.float32
+    ).astype(jnp.bfloat16)
+    reduced = lax.psum_scatter(terms, ("sp", "tp"), scatter_dimension=0, tiled=True)
+    reduced = widened(reduced.astype(jnp.float32))
+    return (stream_wide + rms_norm(reduced, ffn_gain)).astype(jnp.bfloat16)
 
 
 def body(
@@ -120,9 +149,13 @@
         jnp.float32
     )
     stream_wide = widened(own_rows + rms_norm(widened(summed), post_gain))
-    inputs = lax.all_gather(
-        rms_norm(stream_wide, pre_gain).astype(jnp.bfloat16), "tp", axis=0, tiled=True
-    )
+    own_inputs = rms_norm(stream_wide, pre_gain).astype(jnp.bfloat16)
+    sp_size = lax.axis_size("sp")
+    if up_value.shape[1] // sp_size >= 128:
+        return feed_by_units(
+            own_inputs, stream_wide, up_value, up_gate, conv_value, conv_gate, down_weight, ffn_gain
+        )
+    inputs = lax.all_gather(own_inputs, "tp", axis=0, tiled=True)
     ff_dev = up_value.shape[1]
     up_joined = jnp.concatenate([up_value, up_gate], axis=1)
     up_whole = lax.all_gather(up_joined, "sp", axis=0, tiled=True)

time: 554 us -> 387 us (0.70)
  waiting for transfers between devices: 436 us -> 249 us
  starting transfers between devices: 4.99 us -> 21.3 us
    all_gather x2 -> x1, waiting for transfers between devices: 410 us -> 42.7 us  [feed_by_units(): inputs = lax.all_gather(own_inputs, ('sp', 'tp'), axis=0, tiled=True)]
    reduce_scatter x1, waiting for transfers between devices: 6.24 us -> 148 us  [feed_by_units(): lax.psum_scatter(terms, ('sp', 'tp'), scatter_dimension=0, tiled=True)]
    all_to_all x0 -> x2, waiting for transfers between devices: none -> 40.4 us  [the longest x1 40.4 us: feed_by_units(): lax.all_to_all(up_pair, 'sp', split_axis=2, concat_axis=1, tiled=True)]
    all_to_all x0 -> x2, starting transfers between devices: none -> 21 us  [the longest x1 14.2 us: feed_by_units(): lax.all_to_all(down_weight, 'sp', split_axis=0, concat_axis=1, tiled=True)]
    dot_general x2 -> x3, matrix products: 18.4 us -> 21.3 us  [the longest x1 11.9 us: feed_by_units(): jnp.dot(hidden.astype(jnp.bfloat16), down_mine, preferred_element_type=jn...]
  transfers between devices with their start and end apart: 7 -> 6, of which waited for: 7 -> 5; matrix products, arithmetic and copies ran while one was open for 4% -> 5% of each run, Pallas kernels for 0% -> 0%
where the time goes in v1:
time: 387 us; the launch traced here: 386 us
  waiting for transfers between devices  249 us (64%)
  blocking collectives  44 us (11%)
  matrix products  33.7 us (9%)
  starting transfers between devices  21.3 us (6%)
  other arithmetic  15.8 us (4%)
  between operations  13.4 us (3%)
  local copies, waits for them, and re-layouts  8.25 us (2%)
    reduce_scatter x1, waiting for transfers between devices, feed_by_units(): lax.psum_scatter(terms, ('sp', 'tp'), scatter_dimension=0, tiled=True)  148 us
    all_gather x1, blocking collectives, body(): lax.all_gather(key_turn, 'sp', axis=0, tiled=True)  44 us
    all_gather x1, waiting for transfers between devices, feed_by_units(): inputs = lax.all_gather(own_inputs, ('sp', 'tp'), axis=0, tiled=True)  42.7 us
    all_to_all x1, waiting for transfers between devices, feed_by_units(): lax.all_to_all(up_pair, 'sp', split_axis=2, concat_axis=1, tiled=True)  40.4 us
    all_to_all x1, starting transfers between devices, feed_by_units(): lax.all_to_all(down_weight, 'sp', split_axis=0, concat_axis=1, tiled=True)  14.2 us
    dot_general x1, matrix products, feed_by_units(): jnp.dot(hidden.astype(jnp.bfloat16), down_mine, preferred_element_type=jn...  11.9 us
    all_gather x1, waiting for transfers between devices, body(): lax.all_gather(normed, 'sp', axis=0, tiled=True)  10.8 us
    dot_general x2, matrix products, conved(): jnp.dot(inputs, weight, preferred_element_type=jnp.float32)  9.39 us
  transfers between devices with their start and end apart: 6, of which 5 were waited for; matrix products, arithmetic and copies ran while one was open for 5% of the time, Pallas kernels for 0%

profile of v1, /device:TPU:0, one launch (start us, length us, event | category | flops | bytes accessed | tf_op | source)
XLA Modules:
  0.0 385.8 jit_solution(14589886979712655266)
XLA Ops:
  6.5 1.1 fusion.55
  7.7 0.7 convert_element_type.120
  8.3 1.6 fusion.57
  9.9 0.0 reduce-scatter.3.cloned.1.call-start
  10.0 0.9 convert.19
  10.8 0.7 convert.18
  11.6 0.1 fusion.64
  11.8 0.1 multiply_cosine_fusion
  11.9 44.0 %all_gather.10 = bf16[2048,64]{0,1:T(8,128)(2,1)S(1)} all-gather(bf16[128,64]{0,1:T(8,128)(2,1)S(1)} %bitcast.80), channel_id=1, replica_groups=mesh['sp'=16,'tp'=2] {'sp'}, dimensions={0}, use_global_device_ids=true | all-gather | bytes 278528 | tf_op jit(solution)/shard_map/all_gather | solution.py:117
  56.0 1.5 constant_dynamic-slice_fusion
  57.5 10.8 %all-gather.3.cloned.1.call-done = bf16[2048,256]{1,0:T(8,128)(2,1)} async-done(((bf16[128,256]{1,0:T(8,128)(2,1)}), bf16[2048,256]{1,0:T(8,128)(2,1)}) %all-gather.3.cloned.1.call-update) | async-done | bytes 1048592 | tf_op jit(solution)/shard_map/all_gather | solution.py:116
  68.3 4.5 %fusion.6 = f32[4,2048,128]{2,1,0:T(8,128)} fusion(bf16[2048,256]{1,0:T(8,128)(2,1)} %all-gather.3.cloned.1.call-done, bf16[256,4,128]{2,1,0:T(4,128)(2,1)S(1)} %get-tuple-element.26, bf16[128,4,128]{2,1,0:T(4,128)(2,1)S(1)} %copy-done.6), kind=kOutput, calls=%fused_computation.13 | convolution fusion | flops 806354944 | bytes 5636096 | tf_op jit(solution)/shard_map/qhd,khd->hqk/dot_general | solution.py:127
  72.8 2.9 fusion.73
  75.7 0.6 fusion.1
  76.3 1.4 copy-done.1
  77.7 0.1 copy-done.4
  77.7 3.8 fusion.19
  81.6 1.3 convolution_convert_fusion.5
  82.9 0.0 all-gather.5.cloned.1.call-start
  83.0 6.8 %reduce-scatter.3.cloned.1.call-done = bf16[64,2048]{1,0:T(8,128)(2,1)} async-done(((bf16[128,2048]{1,0:T(8,128)(2,1)}), bf16[64,2048]{1,0:T(8,128)(2,1)}) %reduce-scatter.3.cloned.1.call-update) | async-done | bytes 262160 | tf_op jit(solution)/shard_map/reduce_scatter | solution.py:142
  89.8 1.1 fusion.40
  90.9 1.1 fusion.43
  92.0 0.2 fusion.46
  92.2 0.5 copy-done.2
  92.7 0.8 fusion.48
  93.6 0.3 copy.32
  94.0 1.5 copy.33
  95.4 0.1 pad_maximum_fusion
  95.6 1.3 copy.34
  96.8 6.7 %all-to-all-start = ((bf16[2,128,16,176]{1,3,0,2:T(8,128)(2,1)}), bf16[2,128,16,176]{1,3,0,2:T(8,128)(2,1)S(1)}, u32[]{:S(2)}, u32[]{:S(2)}) async-start(bf16[2,128,16,176]{1,3,0,2:T(8,128)(2,1)} %copy.34), calls=%async_computation.1 | async-start | bytes 2883584 | tf_op jit(solution)/shard_map/all_to_all | solution.py:66
  103.6 0.8 dynamic-slice_convert_fusion
  104.4 0.5 fusion.72
  104.9 40.4 %all-to-all-done = bf16[2,128,16,176]{1,3,0,2:T(8,128)(2,1)S(1)} async-done(((bf16[2,128,16,176]{1,3,0,2:T(8,128)(2,1)}), bf16[2,128,16,176]{1,3,0,2:T(8,128)(2,1)S(1)}, u32[]{:S(2)}, u32[]{:S(2)}) %all-to-all-start) | async-done | bytes 1441824 | tf_op jit(solution)/shard_map/all_to_all | solution.py:66
  145.3 14.2 %all-to-all-start.1 = ((bf16[16,176,128]{2,1,0:T(8,128)(2,1)}), bf16[16,176,128]{2,1,0:T(8,128)(2,1)}, u32[]{:S(2)}, u32[]{:S(2)}) async-start(bf16[16,176,128]{2,1,0:T(8,128)(2,1)} %bitcast.74), calls=%async_computation.2 | async-start | bytes 1441792 | tf_op jit(solution)/shard_map/all_to_all | solution.py:67
  159.5 0.2 reduce-scatter.5.cloned.1.call-start
  159.8 0.1 fusion.70
  159.9 0.2 copy.36
  160.1 0.2 copy.35
  160.3 42.7 %all-gather.5.cloned.1.call-done = bf16[2048,2048]{1,0:T(8,128)(2,1)} async-done(((bf16[64,2048]{1,0:T(8,128)(2,1)}), bf16[2048,2048]{1,0:T(8,128)(2,1)}) %all-gather.5.cloned.1.call-update) | async-done | bytes 8388624 | tf_op jit(solution)/shard_map/all_gather | solution.py:68
  203.0 6.5 %convolution_convert_fusion.3 = bf16[2048,176]{0,1:T(8,128)(2,1)S(1)} fusion(bf16[2048,2048]{1,0:T(8,128)(2,1)} %all-gather.5.cloned.1.call-done, bf16[22,8,16,128]{3,2,1,0:T(8,128)(2,1)S(1)} %bitcast.76), kind=kOutput, calls=%fused_computation.8 | convolution fusion | flops 1476755456 | bytes 9830400 | tf_op jit(solution)/shard_map/dot_general | solution.py:71
  209.4 1.5 pad_convert_fusion
  210.9 2.9 convolution_convert_fusion.4
  213.8 1.4 pad_convert_fusion.1
  215.3 11.9 %convolution_convert_fusion = bf16[2048,2048]{1,0:T(8,128)(2,1)} fusion(f32[2050,176]{0,1:T(8,128)} %pad_convert_fusion, f32[2050,176]{0,1:T(8,128)} %pad_convert_fusion.1, f32[176]{0:T(256)S(1)} %bitcast.87, f32[176]{0:T(256)S(1)} %bitcast.88, f32[176]{0:T(256)S(1)} %bitcast.86, f32[176]{0:T(256)S(1)} %bitcast.84, f32[176]{0:T(256)S(1)} %bitcast.85, ...), kind=kOutput, calls=%fused_computation | convolution fusion | flops 1486356480 | bytes 17764480 | tf_op jit(solution)/shard_map/dot_general | solution.py:77
  227.1 0.7 copy-done.10
  227.8 148.5 %reduce-scatter.5.cloned.1.call-done = bf16[64,2048]{1,0:T(8,128)(2,1)} async-done(((bf16[2048,2048]{1,0:T(8,128)(2,1)}), bf16[64,2048]{1,0:T(8,128)(2,1)}) %reduce-scatter.5.cloned.1.call-update) | async-done | bytes 262160 | tf_op jit(solution)/shard_map/reduce_scatter | solution.py:80
  376.3 1.1 fusion.44
  377.4 1.8 fusion.49
  (45 shorter events, 0.2 us)
Async XLA Ops:
  6.5 75.0 %copy-start = (bf16[512,2048]{1,0:T(8,128)(2,1)S(1)}, bf16[512,2048]{1,0:T(8,128)(2,1)}, u32[]{:S(2)}) copy-start(bf16[512,2048]{1,0:T(8,128)(2,1)} %param.25) | copy-start | bytes 6291460
  6.5 61.8 %copy-start.6 = (bf16[128,4,128]{2,1,0:T(4,128)(2,1)S(1)}, bf16[128,4,128]{2,1,0:T(4,128)(2,1)}, u32[]{:S(2)}) copy-start(bf16[128,4,128]{2,1,0:T(4,128)(2,1)} %param.18) | copy-start | bytes 393220
  6.5 61.8 %all-gather.3.cloned.1.call-start = ((), (), s32[]{:S(2)}) async-start(), calls=%async_computation.4 | async-start | bytes 1114112 | tf_op jit(solution)/shard_map/all_gather | solution.py:116
  9.9 79.9 %reduce-scatter.3.cloned.1.call-start = ((), (), s32[]{:S(2)}) async-start(), calls=%async_computation.5 | async-start | bytes 786432 | tf_op jit(solution)/shard_map/reduce_scatter | solution.py:142
  75.7 2.0 copy-start.1
  75.7 2.0 copy-start.4
  81.5 1.4 copy-start.8
  81.6 1.4 copy-start.9
  81.6 9.3 %copy-start.7 = (bf16[128,2048]{1,0:T(8,128)(2,1)S(1)}, bf16[128,2048]{1,0:T(8,128)(2,1)}, u32[]{:S(2)}) copy-start(bf16[128,2048]{1,0:T(8,128)(2,1)} %param.17) | copy-start | bytes 1572868
  82.8 10.7 %copy-start.5 = (bf16[128,2816]{1,0:T(8,128)(2,1)S(1)}, bf16[128,2816]{1,0:T(8,128)(2,1)}, u32[]{:S(2)}) copy-start(bf16[128,2816]{1,0:T(8,128)(2,1)} %param.29) | copy-start | bytes 2162692
  82.9 120.1 %all-gather.5.cloned.1.call-start = ((), (), s32[]{:S(2)}) async-start(), calls=%async_computation.6 | async-start | bytes 8650752 | tf_op jit(solution)/shard_map/all_gather | solution.py:68
  92.0 0.7 copy-start.2
  96.8 48.5 %all-to-all-start = ((bf16[2,128,16,176]{1,3,0,2:T(8,128)(2,1)}), bf16[2,128,16,176]{1,3,0,2:T(8,128)(2,1)S(1)}, u32[]{:S(2)}, u32[]{:S(2)}) async-start(bf16[2,128,16,176]{1,3,0,2:T(8,128)(2,1)} %copy.34), calls=%async_computation.1 | async-start | bytes 2883584 | tf_op jit(solution)/shard_map/all_to_all | solution.py:66
  145.3 69.9 %all-to-all-start.1 = ((bf16[16,176,128]{2,1,0:T(8,128)(2,1)}), bf16[16,176,128]{2,1,0:T(8,128)(2,1)}, u32[]{:S(2)}, u32[]{:S(2)}) async-start(bf16[16,176,128]{2,1,0:T(8,128)(2,1)} %bitcast.74), calls=%async_computation.2 | async-start | bytes 1441792 | tf_op jit(solution)/shard_map/all_to_all | solution.py:67
  159.5 216.7 %reduce-scatter.5.cloned.1.call-start = ((), (), s32[]{:S(2)}) async-start(), calls=%async_computation.7 | async-start | bytes 8650752 | tf_op jit(solution)/shard_map/reduce_scatter | solution.py:80
  203.0 7.9 %copy-start.13 = (bf16[2048,2048]{1,0:T(8,128)(2,1)S(1)}, bf16[2048,2048]{1,0:T(8,128)(2,1)}, u32[]{:S(2)}) copy-start(bf16[2048,2048]{1,0:T(8,128)(2,1)} %all-gather.5.cloned.1.call-done) | copy-start | bytes 25165828
  213.8 1.4 copy-start.11
  213.8 1.4 copy-start.12
  227.1 0.7 copy-start.10
  227.1 150.3 %copy-start.3 = (bf16[64,2048]{1,0:T(8,128)(2,1)S(1)}, bf16[64,2048]{1,0:T(8,128)(2,1)}, u32[]{:S(2)}) copy-start(bf16[64,2048]{1,0:T(8,128)(2,1)} %copy-done.2) | copy-start | bytes 786436
Sparse Core Ops, SparseCore 0:
  10.1 58.1 all-gather.2
  83.0 6.7 reduce-scatter.2
  93.7 109.2 all-gather.4
  227.3 148.9 reduce-scatter.4
